TPU v7x, 32 devices: a whole 2x2x4 slice. The times are simulated.
32 devices in a mesh: fs: 4 (over y, x), tp: 8 (over z, core).
Axes of the slice: x: 2, y: 2, z: 4, core: 2. Of those that a mesh axis runs over, the one named last changes fastest.
Arguments:
- features: bfloat16 [8192, 2048], P('fs', 'tp'), may hold values from -6 to 6
- gate_cotangent: bfloat16 [8192, 4096], P('fs', 'tp'), may hold values from -0.059814453 to 0.059814453
- gate_basis: bfloat16 [2048, 128], replicated, may hold values from -0.125 to 0.125
- gate_master: float32 [2048, 4096], P('fs', 'tp'), may hold values from -6 to 6
- gate_first: float32 [128, 4096], P('fs', 'tp'), may hold values from -144 to 144
- gate_second: float32 [128, 4096], P('fs', 'tp'), may hold values from 0.2 to 4
- input_cotangent: bfloat16 [8192, 4096], P('fs', 'tp'), may hold values from -0.059814453 to 0.059814453
- input_basis: bfloat16 [2048, 128], replicated, may hold values from -0.125 to 0.125
- input_master: float32 [2048, 4096], P('fs', 'tp'), may hold values from -6 to 6
- input_first: float32 [128, 4096], P('fs', 'tp'), may hold values from -144 to 144
- input_second: float32 [128, 4096], P('fs', 'tp'), may hold values from 0.2 to 4
- state_cotangent: bfloat16 [8192, 1024], P('fs', 'tp'), may hold values from -0.059814453 to 0.059814453
- state_basis: bfloat16 [2048, 128], replicated, may hold values from -0.125 to 0.125
- state_master: float32 [2048, 1024], P('fs', 'tp'), may hold values from -6 to 6
- state_first: float32 [128, 1024], P('fs', 'tp'), may hold values from -144 to 144
- state_second: float32 [128, 1024], P('fs', 'tp'), may hold values from 0.2 to 4
Outputs:
- gate_update: float32 [2048, 4096], P('fs', 'tp')
- gate_master_next: float32 [2048, 4096], P('fs', 'tp')
- gate_first_next: float32 [128, 4096], P('fs', 'tp')
- gate_second_next: float32 [128, 4096], P('fs', 'tp')
- gate_copy: bfloat16 [2048, 4096], P(None, 'tp')
- input_update: float32 [2048, 4096], P('fs', 'tp')
- input_master_next: float32 [2048, 4096], P('fs', 'tp')
- input_first_next: float32 [128, 4096], P('fs', 'tp')
- input_second_next: float32 [128, 4096], P('fs', 'tp')
- input_copy: bfloat16 [2048, 4096], P(None, 'tp')
- state_update: float32 [2048, 1024], P('fs', 'tp')
- state_master_next: float32 [2048, 1024], P('fs', 'tp')
- state_first_next: float32 [128, 1024], P('fs', 'tp')
- state_second_next: float32 [128, 1024], P('fs', 'tp')
- state_copy: bfloat16 [2048, 1024], P(None, 'tp')
All inputs are finite; a program needn't handle non-finite values.
Results may differ from a plain program's by a relative error of at most 0.001.
Values may be sent and summed in bfloat16 or wider, within the bound.
A program may use at most 64 MiB of HBM per device.

v0:
```python
import jax
import jax.numpy as jnp
from jax import lax
from jax.sharding import PartitionSpec as P


def shards(
    features,
    gate_cotangent,
    gate_basis,
    gate_master,
    gate_first,
    gate_second,
    input_cotangent,
    input_basis,
    input_master,
    input_first,
    input_second,
    state_cotangent,
    state_basis,
    state_master,
    state_first,
    state_second,
):
    cotangents = (gate_cotangent, input_cotangent, state_cotangent)
    bases = (gate_basis, input_basis, state_basis)
    masters = (gate_master, input_master, state_master)
    firsts = (gate_first, input_first, state_first)
    seconds = (gate_second, input_second, state_second)
    widths = [c.shape[1] for c in cotangents]
    rows_dev = gate_master.shape[0]
    row_start = lax.axis_index("fs") * rows_dev
    local_bases = [
        lax.dynamic_slice_in_dim(b, row_start, rows_dev, 0).astype(jnp.float32) for b in bases
    ]
    feat_cols = features.shape[1]
    col_start = lax.axis_index("tp") * feat_cols
    partials = tuple(
        (
            jnp.dot(
                features,
                lax.dynamic_slice_in_dim(b, col_start, feat_cols, 0),
                preferred_element_type=jnp.float32,
            )
            for b in bases
        )
    )
    mapped = lax.psum(partials, "tp")
    terms = [
        lax.dot_general(
            mapped[index],
            cotangents[index].astype(jnp.float32),
            (((0,), (0,)), ((), ())),
            precision=lax.Precision.HIGHEST,
        )
        for index in range(3)
    ]
    projected = (
        lax.psum_scatter(terms[0], "fs", scatter_dimension=0, tiled=True),
        lax.psum_scatter(terms[1], "fs", scatter_dimension=0, tiled=True),
        lax.psum_scatter(terms[2], "fs", scatter_dimension=0, tiled=True),
    )
    first_next = [0.8 * firsts[i] + 0.2 * projected[i] for i in range(3)]
    second_next = [0.9 * seconds[i] + 0.1 * projected[i] * projected[i] for i in range(3)]
    direction = [first_next[i] / jnp.sqrt(second_next[i]) for i in range(3)]
    totals = lax.psum(
        (
            jnp.sum(direction[0] * direction[0]),
            jnp.sum(direction[1] * direction[1]),
            jnp.sum(direction[2] * direction[2]),
        ),
        ("fs", "tp"),
    )
    whole_dir = (
        lax.all_gather(direction[0], "fs", axis=0, tiled=True),
        lax.all_gather(direction[1], "fs", axis=0, tiled=True),
        lax.all_gather(direction[2], "fs", axis=0, tiled=True),
    )
    results = []
    copies_in = []
    for index in range(3):
        entries = whole_dir[index].shape[0] * widths[index] * lax.axis_size("tp")
        scale = lax.rsqrt(totals[index] / entries + 1e-06)
        update = (
            jnp.dot(local_bases[index], whole_dir[index], precision=lax.Precision.HIGHEST) * scale
        )
        master_next = masters[index] - 0.05 * update
        results.append((update, master_next))
        copies_in.append(master_next.astype(jnp.bfloat16))
    copies = (
        lax.all_gather(copies_in[0], "fs", axis=0, tiled=True),
        lax.all_gather(copies_in[1], "fs", axis=0, tiled=True),
        lax.all_gather(copies_in[2], "fs", axis=0, tiled=True),
    )
    return (
        results[0][0],
        results[0][1],
        first_next[0],
        second_next[0],
        copies[0],
        results[1][0],
        results[1][1],
        first_next[1],
        second_next[1],
        copies[1],
        results[2][0],
        results[2][1],
        first_next[2],
        second_next[2],
        copies[2],
    )


def solution(mesh):
    placed = (
        P("fs", "tp"),
        P("fs", "tp"),
        P(),
        P("fs", "tp"),
        P("fs", "tp"),
        P("fs", "tp"),
        P("fs", "tp"),
        P(),
        P("fs", "tp"),
        P("fs", "tp"),
        P("fs", "tp"),
        P("fs", "tp"),
        P(),
        P("fs", "tp"),
        P("fs", "tp"),
        P("fs", "tp"),
    )
    return jax.shard_map(
        shards,
        mesh=mesh,
        in_specs=placed,
        out_specs=(
            P("fs", "tp"),
            P("fs", "tp"),
            P("fs", "tp"),
            P("fs", "tp"),
            P(None, "tp"),
            P("fs", "tp"),
            P("fs", "tp"),
            P("fs", "tp"),
            P("fs", "tp"),
            P(None, "tp"),
            P("fs", "tp"),
            P("fs", "tp"),
            P("fs", "tp"),
            P("fs", "tp"),
            P(None, "tp"),
        ),
        check_vma=False,
    )
```

profile of v0, /device:TPU:0, one launch (start us, length us, event | category | flops | bytes accessed | tf_op | source)
XLA Modules:
  0.0 320.3 jit_solution(3908073077434583546)
XLA Ops:
  7.3 2.9 convolution_bitcast_fusion.2
  10.2 2.3 convolution_bitcast_fusion.1
  12.5 2.3 convolution_bitcast_fusion
  14.8 79.8 %all-reduce.4.cloned.1.call-done = (f32[2048,128]{0,1:T(8,128)}, f32[2048,128]{0,1:T(8,128)}, f32[2048,128]{0,1:T(8,128)}) async-done(((f32[2048,128]{0,1:T(8,128)}, f32[2048,128]{0,1:T(8,128)}, f32[2048,128]{0,1:T(8,128)}), (f32[2048,128]{0,1:T(8,128)}, f32[2048,128]{0,1:T(8,128)}, f32[2048,128]{0,1:T(8,128)})) %all-reduce.4.cloned.1.call-update) | async-done | bytes 3145744 | tf_op jit(solution)/shard_map/psum | solution.py:48
  94.6 2.7 fusion.23
  97.4 1.7 fusion.21
  99.2 3.7 %fusion.22 = f32[128,512]{1,0:T(8,128)} fusion(f32[2048,128]{0,1:T(8,128)} %get-tuple-element.19, bf16[2048,512]{1,0:T(8,128)(2,1)} %param.22), kind=kOutput, calls=%fused_computation.40 | convolution fusion | flops 1610612736 | bytes 3407872 | tf_op jit(solution)/shard_map/dot_general | solution.py:50
  103.0 18.8 %reduce-scatter.8.cloned.1.call-done = f32[32,128]{1,0:T(8,128)} async-done(((f32[128,128]{1,0:T(8,128)}), f32[32,128]{1,0:T(8,128)}) %reduce-scatter.8.cloned.1.call-update) | async-done | bytes 16400 | tf_op jit(solution)/shard_map/reduce_scatter | solution.py:61
  121.9 1.9 multiply_reduce_fusion.2
  123.8 25.8 %reduce-scatter.4.cloned.1.call-done = f32[32,512]{1,0:T(8,128)} async-done(((f32[128,512]{1,0:T(8,128)}), f32[32,512]{1,0:T(8,128)}) %reduce-scatter.4.cloned.1.call-update) | async-done | bytes 65552 | tf_op jit(solution)/shard_map/reduce_scatter | solution.py:59
  149.6 2.1 multiply_reduce_fusion.1
  151.7 25.4 %reduce-scatter.6.cloned.1.call-done = f32[32,512]{1,0:T(8,128)} async-done(((f32[128,512]{1,0:T(8,128)}), f32[32,512]{1,0:T(8,128)}) %reduce-scatter.6.cloned.1.call-update) | async-done | bytes 65552 | tf_op jit(solution)/shard_map/reduce_scatter | solution.py:60
  177.2 2.1 multiply_reduce_fusion
  179.3 39.6 %all-reduce = (f32[]{:T(128)}, f32[]{:T(128)}, f32[]{:T(128)}) all-reduce(f32[]{:T(128)} %get-tuple-element.35, f32[]{:T(128)} %get-tuple-element.31, f32[]{:T(128)} %get-tuple-element.27), channel_id=1, replica_groups=mesh['fs'=4,'tp'=8] {'fs','tp'}, use_global_device_ids=true, to_apply=%region_3.0 | all-reduce | flops 3 | bytes 24 | tf_op jit(solution)/shard_map/psum | solution.py:66
  219.5 10.3 %all_gather.18 = f32[128,512]{1,0:T(8,128)S(1)} all-gather(f32[32,512]{1,0:T(8,128)S(1)} %get-tuple-element.36), channel_id=1, replica_groups=mesh['fs'=4,'tp'=8] {'fs'}, dimensions={0}, use_global_device_ids=true | all-gather | bytes 327680 | tf_op jit(solution)/shard_map/all_gather | solution.py:75
  229.8 3.1 fusion.17
  233.7 9.3 %all_gather.20 = f32[128,512]{1,0:T(8,128)S(1)} all-gather(f32[32,512]{1,0:T(8,128)S(1)} %get-tuple-element.32), channel_id=1, replica_groups=mesh['fs'=4,'tp'=8] {'fs'}, dimensions={0}, use_global_device_ids=true | all-gather | bytes 327680 | tf_op jit(solution)/shard_map/all_gather | solution.py:76
  243.0 3.5 %fusion.16 = (bf16[512,512]{1,0:T(8,128)(2,1)}, f32[512,512]{1,0:T(8,128)}, f32[512,512]{1,0:T(8,128)}) fusion(f32[512,512]{1,0:T(8,128)} %param.24, f32[]{:T(128)S(6)} %rsqrt.13, f32[128,512]{1,0:T(8,128)S(1)} %all_gather.20, bf16[2048,128]{1,0:T(8,128)(2,1)} %param.23, s32[]{:T(128)S(6)} %select_n.4), kind=kOutput, calls=%fused_computation.37 | convolution fusion | flops 403701760 | bytes 4063240 | tf_op jit(solution)/shard_map/dot_general | solution.py:85
  246.5 7.9 %all_gather.22 = f32[128,128]{1,0:T(8,128)S(1)} all-gather(f32[32,128]{1,0:T(8,128)S(1)} %get-tuple-element.28), channel_id=1, replica_groups=mesh['fs'=4,'tp'=8] {'fs'}, dimensions={0}, use_global_device_ids=true | all-gather | bytes 81920 | tf_op jit(solution)/shard_map/all_gather | solution.py:77
  255.1 2.0 fusion.15
  257.0 13.6 %all_gather.23 = bf16[2048,128]{1,0:T(8,128)(2,1)S(1)} all-gather(bf16[512,128]{1,0:T(8,128)(2,1)S(1)} %get-tuple-element.21), channel_id=1, replica_groups=mesh['fs'=4,'tp'=8] {'fs'}, dimensions={0}, use_global_device_ids=true | all-gather | bytes 655360 | tf_op jit(solution)/shard_map/all_gather | solution.py:93
  271.1 37.0 %all-gather.5.cloned.1.call-done = bf16[2048,512]{1,0:T(8,128)(2,1)} async-done(((bf16[512,512]{1,0:T(8,128)(2,1)}), bf16[2048,512]{1,0:T(8,128)(2,1)}) %all-gather.5.cloned.1.call-update) | async-done | bytes 2097168 | tf_op jit(solution)/shard_map/all_gather | solution.py:92
  308.1 3.2 copy.37
  311.3 1.3 copy.38
  (38 shorter events, 1.6 us)
Async XLA Ops:
  7.2 90.2 %copy-start = (bf16[2048,512]{1,0:T(8,128)(2,1)S(1)}, bf16[2048,512]{1,0:T(8,128)(2,1)}, u32[]{:S(2)}) copy-start(bf16[2048,512]{1,0:T(8,128)(2,1)} %param.17) | copy-start | bytes 6291460
  7.2 3.0 copy-start.1
  7.2 87.4 %all-reduce.4.cloned.1.call-start = ((), (), s32[]{:S(2)}) async-start(), calls=%async_computation.8 | async-start | bytes 6291456 | tf_op jit(solution)/shard_map/psum | solution.py:48
  14.8 107.1 %reduce-scatter.8.cloned.1.call-start = ((), (), s32[]{:S(2)}) async-start(), calls=%async_computation.7 | async-start | bytes 81920 | tf_op jit(solution)/shard_map/reduce_scatter | solution.py:61
  94.6 2.8 copy-start.4
  97.3 52.3 %reduce-scatter.4.cloned.1.call-start = ((), (), s32[]{:S(2)}) async-start(), calls=%async_computation.3 | async-start | bytes 327680 | tf_op jit(solution)/shard_map/reduce_scatter | solution.py:59
  99.1 22.8 %copy-start.10 = (f32[32,128]{1,0:T(8,128)S(1)}, f32[32,128]{1,0:T(8,128)}, u32[]{:S(2)}) copy-start(f32[32,128]{1,0:T(8,128)} %param.31) | copy-start | bytes 49156
  99.1 22.8 %copy-start.11 = (f32[32,128]{1,0:T(8,128)S(1)}, f32[32,128]{1,0:T(8,128)}, u32[]{:S(2)}) copy-start(f32[32,128]{1,0:T(8,128)} %param.30) | copy-start | bytes 49156
  99.1 50.5 %copy-start.6 = (f32[32,512]{1,0:T(8,128)S(1)}, f32[32,512]{1,0:T(8,128)}, u32[]{:S(2)}) copy-start(f32[32,512]{1,0:T(8,128)} %param.21) | copy-start | bytes 196612
  99.1 50.5 %copy-start.7 = (f32[32,512]{1,0:T(8,128)S(1)}, f32[32,512]{1,0:T(8,128)}, u32[]{:S(2)}) copy-start(f32[32,512]{1,0:T(8,128)} %param.20) | copy-start | bytes 196612
  99.2 78.0 %copy-start.8 = (f32[32,512]{1,0:T(8,128)S(1)}, f32[32,512]{1,0:T(8,128)}, u32[]{:S(2)}) copy-start(f32[32,512]{1,0:T(8,128)} %param.26) | copy-start | bytes 196612
  99.2 78.0 %copy-start.9 = (f32[32,512]{1,0:T(8,128)S(1)}, f32[32,512]{1,0:T(8,128)}, u32[]{:S(2)}) copy-start(f32[32,512]{1,0:T(8,128)} %param.25) | copy-start | bytes 196612
  99.2 78.0 %reduce-scatter.6.cloned.1.call-start = ((), (), s32[]{:S(2)}) async-start(), calls=%async_computation.5 | async-start | bytes 327680 | tf_op jit(solution)/shard_map/reduce_scatter | solution.py:60
  99.2 130.6 %copy-start.3 = (f32[512,512]{1,0:T(8,128)S(1)}, f32[512,512]{1,0:T(8,128)}, u32[]{:S(2)}) copy-start(f32[512,512]{1,0:T(8,128)} %param.19) | copy-start | bytes 3145732
  103.0 168.1 %all-gather.3.cloned.1.call-start = ((), (), s32[]{:S(2)}) async-start(), calls=%async_computation.4 | async-start | bytes 2621440 | tf_op jit(solution)/shard_map/all_gather | solution.py:91
  232.9 75.2 %all-gather.5.cloned.1.call-start = ((), (), s32[]{:S(2)}) async-start(), calls=%async_computation.6 | async-start | bytes 2621440 | tf_op jit(solution)/shard_map/all_gather | solution.py:92
  243.0 12.1 %copy-start.5 = (f32[512,128]{1,0:T(8,128)S(1)}, f32[512,128]{1,0:T(8,128)}, u32[]{:S(2)}) copy-start(f32[512,128]{1,0:T(8,128)} %param.29) | copy-start | bytes 786436
  308.1 3.2 copy-start.2
Sparse Core Ops, SparseCore 0:
  14.9 79.6 all-reduce.3
  97.9 23.9 reduce-scatter.7
  125.2 24.3 reduce-scatter.3
  152.8 24.3 reduce-scatter.5
  233.0 37.9 all-gather.2
  273.3 34.7 all-gather.4
where the time goes:
time: 321 us; the launch traced here: 320 us
  waiting for transfers between devices  187 us (58%)
  blocking collectives  80.7 us (25%)
  matrix products  24.1 us (8%)
  between operations  16.3 us (5%)
  other arithmetic  6.15 us (2%)
  local copies, waits for them, and re-layouts  5.36 us (2%)
    psum x1, waiting for transfers between devices, shards(): mapped = lax.psum(partials, 'tp')  79.8 us
    psum x1, blocking collectives, shards(): lax.psum((jnp.sum(direction[0] * direction[0]), jnp.sum(direction[1] * di...  39.6 us
    all_gather x1, waiting for transfers between devices, shards(): lax.all_gather(copies_in[1], 'fs', axis=0, tiled=True)  37 us
    reduce_scatter x1, waiting for transfers between devices, shards(): lax.psum_scatter(terms[0], 'fs', scatter_dimension=0, tiled=True)  25.8 us
    reduce_scatter x1, waiting for transfers between devices, shards(): lax.psum_scatter(terms[1], 'fs', scatter_dimension=0, tiled=True)  25.4 us
    reduce_scatter x1, waiting for transfers between devices, shards(): lax.psum_scatter(terms[2], 'fs', scatter_dimension=0, tiled=True)  18.8 us
    all_gather x1, blocking collectives, shards(): lax.all_gather(copies_in[2], 'fs', axis=0, tiled=True)  13.6 us
    all_gather x1, blocking collectives, shards(): lax.all_gather(direction[0], 'fs', axis=0, tiled=True)  10.3 us
  transfers between devices with their start and end apart: 6, of which 6 were waited for; matrix products, arithmetic and copies ran while one was open for 5% of the time, Pallas kernels for 0%

commit v1 on v0

v1 whole, which is shorter than its diff:
```python
import functools

import jax
import jax.numpy as jnp
from jax import lax
from jax.experimental import pallas as pl
from jax.experimental.pallas import tpu as pltpu
from jax.sharding import PartitionSpec as P

MESH = pl.DeviceIdType.MESH
PIECES = 4
SKEW = 2
F32, BF16 = jnp.float32, jnp.bfloat16


def kernel(n, tp, *refs):
    feat_in = refs[0]
    cot_in, basis_in, master_in, first_in, second_in = (refs[1 + i : 16 : 5] for i in range(5))
    upd_out, mas_out, fir_out, sec_out, cop_out = (refs[16 + i : 31 : 5] for i in range(5))
    (feat, fsib, cot, basis, master, first, second, parts, up_in, dn_in, up_snd, dn_snd,
     tot, sib, proj, rs_in, direction, sums, upd, mas, fir, sec, cop,
     load_sem, store_sem, z_send, z_recv, sib_send, sib_recv, rs_send, rs_recv,
     ag_send, ag_recv, sq_send, sq_recv, bulk_send, bulk_recv) = (
        refs[31], refs[32], refs[33:36], refs[36:39], refs[39:42], refs[42:45], refs[45:48],
        *refs[48:53], refs[53], refs[54], refs[55:58], refs[58:61], refs[61:64], refs[64],
        refs[65:68], refs[68:71], refs[71:74], refs[74:77], refs[77:80], *refs[80:])

    f, t = lax.axis_index("fs"), lax.axis_index("tp")
    zs = tp // 2
    z, c = t // 2, lax.rem(t, 2)
    mate = 2 * z + 1 - c
    half = feat.shape[0]
    width = feat.shape[1]
    rows_dev = master[0].shape[0]
    rank = proj[0].shape[0]
    rb = rank // n
    piece = half // PIECES
    count = 3 * PIECES
    sends = []

    def remote(src, dst, ssem, rsem, **dev):
        return pltpu.make_async_remote_copy(
            src_ref=src, dst_ref=dst, send_sem=ssem, recv_sem=rsem, device_id=dev, device_id_type=MESH
        )

    def load(src, dst, i):
        cp = pltpu.make_async_copy(src, dst, load_sem.at[i])
        cp.start()
        return cp

    my_half = pl.multiple_of(c * half, half)
    mate_half = pl.multiple_of((1 - c) * half, half)
    loads = [load(feat_in.at[pl.ds(my_half, half)], feat, 0)]
    loads += [load(basis_in[k], basis[k], 1 + k) for k in range(3)]
    loads += [load(cot_in[k], cot[k], 4 + k) for k in range(3)]
    loads += [load(first_in[k], first[k], 7 + k) for k in range(3)]
    loads += [load(second_in[k], second[k], 10 + k) for k in range(3)]
    loads += [load(master_in[k], master[k], 13 + k) for k in range(3)]

    barrier = pltpu.get_barrier_semaphore()
    for d in range(1, n):
        pl.semaphore_signal(barrier, inc=1, device_id={"fs": lax.rem(f + d, n)}, device_id_type=MESH)
    for d in range(1, tp):
        pl.semaphore_signal(barrier, inc=1, device_id={"tp": lax.rem(t + d, tp)}, device_id_type=MESH)
    pl.semaphore_wait(barrier, n + tp - 2)

    share = remote(feat_in.at[pl.ds(mate_half, half)], fsib, sib_send.at[3], sib_recv.at[3], tp=mate)
    share.start()

    @pl.when(z == 0)
    def _():
        up_in[...] = jnp.zeros_like(up_in)

    @pl.when(z == zs - 1)
    def _():
        dn_in[...] = jnp.zeros_like(dn_in)

    for cp in loads[:4]:
        cp.wait()
    mine = pl.ds(pl.multiple_of(t * width, width), width)
    theirs = pl.ds(pl.multiple_of(mate * width, width), width)
    share.wait()
    for k in range(3):
        own = jnp.dot(feat[...], basis[k][mine, :], preferred_element_type=F32)
        own += jnp.dot(fsib[...], basis[k][theirs, :], preferred_element_type=F32)
        for j in range(PIECES):
            parts[k * PIECES + j] = own[j * piece : (j + 1) * piece]

    def hop(j, has_src, has_dst, src_in, snd, lane, to):
        @pl.when((j >= 0) & (j < count))
        def _():
            jj = jnp.clip(j, 0, count - 1)
            copy = remote(snd.at[jj], src_in.at[jj], z_send.at[lane, jj], z_recv.at[lane, jj], tp=to)

            @pl.when(has_src)
            def _():
                copy.wait_recv()

            @pl.when(has_dst)
            def _():
                snd[jj] = (parts[jj] + src_in[jj].astype(F32)).astype(BF16)
                copy.start()

    above = jnp.minimum(t + 2, tp - 2 + c)
    below = jnp.maximum(t - 2, c)

    def z_step(step):
        hop(step - SKEW * z, z > 0, z < zs - 1, up_in, up_snd, 0, above)
        hop(step - SKEW * (zs - 1 - z), z < zs - 1, z > 0, dn_in, dn_snd, 1, below)

    mate_copy = [remote(tot.at[k], sib.at[k], sib_send.at[k], sib_recv.at[k], tp=mate) for k in range(3)]

    def act_total(k):
        for j in range(PIECES):
            i = k * PIECES + j
            whole = parts[i] + up_in[i].astype(F32) + dn_in[i].astype(F32)
            tot[k, j * piece : (j + 1) * piece, :] = whole.astype(BF16)
        mate_copy[k].start()

    def contract(a, b):
        return lax.dot_general(a, b, (((0,), (0,)), ((), ())), preferred_element_type=F32)

    def rows_of(i):
        return pl.ds(pl.multiple_of(i * rb, rb), rb)

    def rs_copy(k, d):
        peer = lax.rem(f + d, n)
        return remote(proj[k].at[rows_of(peer)], rs_in[k].at[d - 1], rs_send.at[k, d - 1], rs_recv.at[k, d - 1], fs=peer)

    def ag_copy(k, d, whose):
        peer = lax.rem(f + d, n)
        r = direction[k].at[rows_of(whose)]
        return remote(r, r, ag_send.at[k, d - 1], ag_recv.at[k, d - 1], fs=peer)

    def sq_copy(k, d, whose):
        peer = lax.rem(t + d, tp)
        r = sums.at[k, whose]
        return remote(r, r, sq_send.at[k, d - 1], sq_recv.at[k, d - 1], tp=peer)

    def act_project(k):
        loads[4 + k].wait()
        acc = contract(tot[k], cot[k][pl.ds(my_half, half), :])
        mate_copy[k].wait_recv()
        proj[k][...] = acc + contract(sib[k], cot[k][pl.ds(mate_half, half), :])
        for d in range(1, n):
            rs_copy(k, d).start()

    def store(src, dst, k, i):
        cp = pltpu.make_async_copy(src, dst, store_sem.at[k, i])
        cp.start()
        sends.append(cp.wait)

    def act_moment(k):
        loads[7 + k].wait()
        loads[10 + k].wait()
        r = proj[k][rows_of(f), :]
        for d in range(1, n):
            rs_copy(k, d).wait_recv()
            r = r + rs_in[k][d - 1]
        a = 0.8 * first[k][...] + 0.2 * r
        b = 0.9 * second[k][...] + 0.1 * r * r
        fir[k][...] = a
        sec[k][...] = b
        direction[k][rows_of(f), :] = a / jnp.sqrt(b)
        for d in range(1, n):
            ag_copy(k, d, f).start()
        store(fir[k], fir_out[k], k, 0)
        store(sec[k], sec_out[k], k, 1)

    rows = pl.ds(pl.multiple_of(f * rows_dev, rows_dev), rows_dev)

    def act_direction(k):
        for d in range(1, n):
            ag_copy(k, d, lax.rem(f - d + n, n)).wait_recv()
        whole = direction[k][...]
        sums[k, t] = jnp.full((8, 128), jnp.sum(whole * whole), F32)
        for d in range(1, tp):
            sq_copy(k, d, t).start()
        high = whole.astype(BF16)
        low = (whole - high.astype(F32)).astype(BF16)
        base = basis[k][rows, :]
        upd[k][...] = jnp.dot(
            jnp.concatenate([base, base], axis=1),
            jnp.concatenate([high, low], axis=0),
            preferred_element_type=F32,
        )

    hrow = rows_dev // 2

    def block(k, owner, h):
        return cop[k].at[pl.ds(pl.multiple_of(owner * rows_dev + h * hrow, hrow), hrow)]

    def out_block(k, owner, h):
        return cop_out[k].at[pl.ds(pl.multiple_of(owner * rows_dev + h * hrow, hrow), hrow)]

    x_peer = f + 1 - 2 * lax.rem(f, 2)
    y_peer = lax.rem(f + 2, 4)
    diag = lax.rem(x_peer + 2, 4)

    def bulk(k, lane, owner, h, to):
        b = block(k, owner, h)
        return remote(b, b, bulk_send.at[k, lane], bulk_recv.at[k, lane], fs=to)

    def act_finish(k):
        loads[13 + k].wait()
        for d in range(1, tp):
            sq_copy(k, d, lax.rem(t - d + tp, tp)).wait_recv()
        total = jnp.sum(sums[k], axis=0)[0:1, 0:1]
        entries = rank * upd[k].shape[1] * tp
        scale = lax.rsqrt(total / entries + 1e-06)
        update = upd[k][...] * scale
        upd[k][...] = update
        new = master[k][...] - 0.05 * update
        mas[k][...] = new
        cop[k][rows, :] = new.astype(BF16)
        if n == 4:
            for h in range(2):
                bulk(k, h, f, h, x_peer).start()
                bulk(k, 3 - h, f, 1 - h, y_peer).start()
        else:
            for d in range(1, n):
                for h in range(2):
                    bulk(k, 2 * (d - 1) + h, f, h, lax.rem(f + d, n)).start()
        store(upd[k], upd_out[k], k, 2)
        store(mas[k], mas_out[k], k, 3)
        for h in range(2):
            store(block(k, f, h), out_block(k, f, h), k, 4 + h)

    def act_forward(k):
        if n == 4:
            bulk(k, 0, x_peer, 0, x_peer).wait_recv()
            bulk(k, 4, x_peer, 0, y_peer).start()
            bulk(k, 3, y_peer, 1, y_peer).wait_recv()
            bulk(k, 5, y_peer, 1, x_peer).start()
            store(block(k, x_peer, 0), out_block(k, x_peer, 0), k, 6)
            store(block(k, y_peer, 1), out_block(k, y_peer, 1), k, 7)

    def act_arrive(k):
        if n == 4:
            for i, (lane, owner, h) in enumerate(((1, x_peer, 1), (2, y_peer, 0), (4, diag, 0), (5, diag, 1))):
                bulk(k, lane, owner, h, x_peer).wait_recv()
                store(block(k, owner, h), out_block(k, owner, h), k, 8 + i)
        else:
            for d in range(1, n):
                for h in range(2):
                    owner = lax.rem(f - d + n, n)
                    lane = 2 * (d - 1) + h
                    bulk(k, lane, owner, h, owner).wait_recv()
                    store(block(k, owner, h), out_block(k, owner, h), k, 6 + lane)

    todo = {}
    for k in range(3):
        base = (k + 1) * PIECES - 1 + SKEW * (zs - 1)
        for after, act in ((0, act_total), (1, act_project), (3, act_moment), (5, act_direction), (7, act_finish), (12, act_forward)):
            todo.setdefault(base + after, []).append((act, k))
    steps = count + SKEW * (zs - 1)
    for step in range(max(max(todo) + 1, steps)):
        if step < steps:
            z_step(step)
        for act, k in todo.get(step, ()):
            act(k)
    for k in range(3):
        act_arrive(k)

    for wait in sends:
        wait()
    for k in range(3):
        mate_copy[k].wait_send()
        for d in range(1, n):
            rs_copy(k, d).wait_send()
            ag_copy(k, d, f).wait_send()
        for d in range(1, tp):
            sq_copy(k, d, t).wait_send()
        if n == 4:
            for h in range(2):
                bulk(k, h, f, h, x_peer).wait_send()
                bulk(k, 3 - h, f, 1 - h, y_peer).wait_send()
            bulk(k, 4, x_peer, 0, y_peer).wait_send()
            bulk(k, 5, y_peer, 1, x_peer).wait_send()
        else:
            for d in range(1, n):
                for h in range(2):
                    bulk(k, 2 * (d - 1) + h, f, h, lax.rem(f + d, n)).wait_send()
    for j in range(count):
        @pl.when(z < zs - 1)
        def _():
            remote(up_snd.at[j], up_in.at[j], z_send.at[0, j], z_recv.at[0, j], tp=above).wait_send()

        @pl.when(z > 0)
        def _():
            remote(dn_snd.at[j], dn_in.at[j], z_send.at[1, j], z_recv.at[1, j], tp=below).wait_send()


def shards(n, tp, *args):
    features = args[0]
    cots, bases, masters, firsts, seconds = (args[1 + i : 16 : 5] for i in range(5))
    tokens, width = features.shape
    rank = bases[0].shape[1]
    rows_dev = masters[0].shape[0]
    whole_rows = rows_dev * n
    half = tokens // 2
    count = 3 * PIECES
    piece = half // PIECES
    cols = [a.shape[1] for a in cots]

    outs = []
    for k in range(3):
        outs += [
            jax.ShapeDtypeStruct(masters[k].shape, F32),
            jax.ShapeDtypeStruct(masters[k].shape, F32),
            jax.ShapeDtypeStruct(firsts[k].shape, F32),
            jax.ShapeDtypeStruct(firsts[k].shape, F32),
            jax.ShapeDtypeStruct((whole_rows, cols[k]), BF16),
        ]
    like = lambda arrays: [pltpu.VMEM(a.shape, a.dtype) for a in arrays]
    lanes = 6 if n == 4 else 2 * (n - 1)
    dma = lambda *shape: pltpu.SemaphoreType.DMA(shape)
    scratch = (
        [pltpu.VMEM((half, width), BF16)] * 2
        + like(cots)
        + like(bases)
        + like(masters)
        + like(firsts)
        + like(seconds)
        + [pltpu.VMEM((count, piece, rank), F32)]
        + [pltpu.VMEM((count, piece, rank), BF16)] * 4
        + [pltpu.VMEM((3, half, rank), BF16)] * 2
        + [pltpu.VMEM((rank, w), F32) for w in cols]
        + [pltpu.VMEM((n - 1, rank // n, w), F32) for w in cols]
        + [pltpu.VMEM((rank, w), F32) for w in cols]
        + [pltpu.VMEM((3, tp, 8, 128), F32)]
        + like(masters)
        + like(masters)
        + like(firsts)
        + like(firsts)
        + [pltpu.VMEM((whole_rows, w), BF16) for w in cols]
        + [dma(16), dma(3, 6 + max(6, 2 * (n - 1))), dma(2, count), dma(2, count), dma(4), dma(4)]
        + [dma(3, n - 1)] * 4
        + [dma(3, tp - 1)] * 2
        + [dma(3, lanes)] * 2
    )
    return pl.pallas_call(
        functools.partial(kernel, n, tp),
        out_shape=outs,
        in_specs=[pl.BlockSpec(memory_space=pl.ANY)] * 16,
        out_specs=[pl.BlockSpec(memory_space=pl.ANY)] * 15,
        scratch_shapes=scratch,
        compiler_params=pltpu.CompilerParams(
            collective_id=0, has_side_effects=True, vmem_limit_bytes=60 * 1024 * 1024
        ),
    )(*args)


def solution(mesh):
    split = P("fs", "tp")
    return jax.shard_map(
        functools.partial(shards, mesh.shape["fs"], mesh.shape["tp"]),
        mesh=mesh,
        in_specs=(split,) + (split, P(), split, split, split) * 3,
        out_specs=(split, split, split, split, P(None, "tp")) * 3,
        check_vma=False,
    )
```

time: 321 us -> 110 us (0.34)
  waiting for transfers between devices: 187 us -> 0 us
  Pallas kernels: 0 us -> 94.3 us
  blocking collectives: 80.7 us -> 0 us
  matrix products: 24.1 us -> 0 us
  between operations: 16.3 us -> 0.73 us
  local copies, waits for them, and re-layouts: 5.36 us -> 14.6 us
  other arithmetic: 6.15 us -> 0 us
    pallas_call x0 -> x1, Pallas kernels: none -> 94.3 us  [shards(): pl.pallas_call(functools.partial(kernel, n, tp), out_shape=outs, in_specs...]
    psum x1 -> x0, waiting for transfers between devices: 79.8 us -> none  [shards(): mapped = lax.psum(partials, 'tp')]
    reduce_scatter x3 -> x0, waiting for transfers between devices: 70.1 us -> none  [the longest x1 25.8 us: shards(): lax.psum_scatter(terms[0], 'fs', scatter_dimension=0, tiled=True)]
    all_gather x4 -> x0, blocking collectives: 41.1 us -> none  [the longest x1 13.6 us: shards(): lax.all_gather(copies_in[2], 'fs', axis=0, tiled=True)]
    psum x1 -> x0, blocking collectives: 39.6 us -> none  [shards(): lax.psum((jnp.sum(direction[0] * direction[0]), jnp.sum(direction[1] * di...]
    all_gather x2 -> x0, waiting for transfers between devices: 37.4 us -> none  [the longest x1 37 us: shards(): lax.all_gather(copies_in[1], 'fs', axis=0, tiled=True)]
    dot_general x9 -> x0, matrix products: 24.1 us -> none  [the longest x3 8.52 us: shards(): jnp.dot(local_bases[index], whole_dir[index], precision=lax.Precision.HIG...]
    unnamed x27 -> x43, local copies, waits for them, and re-layouts: 5.36 us -> 14.6 us
  transfers between devices with their start and end apart: 6 -> 0, of which waited for: 6 -> 0; matrix products, arithmetic and copies ran while one was open for 5% -> 0% of each run, Pallas kernels for 0% -> 0%
where the time goes in v1:
time: 110 us
  Pallas kernels  94.3 us (86%)
  local copies, waits for them, and re-layouts  14.6 us (13%)
    pallas_call x1, Pallas kernels, shards(): pl.pallas_call(functools.partial(kernel, n, tp), out_shape=outs, in_specs...  94.3 us
    unnamed x43, local copies, waits for them, and re-layouts  14.6 us

profile of v1, /device:TPU:0, one launch (start us, length us, event | category | flops | bytes accessed | tf_op | source)
XLA Modules:
  0.0 109.6 jit_solution(527772986225139143)
XLA Ops:
  0.7 94.3 %shard_map.271 = (f32[512,512]{1,0:T(8,128)}, f32[512,512]{1,0:T(8,128)}, f32[32,512]{1,0:T(8,128)}, f32[32,512]{1,0:T(8,128)}, bf16[2048,512]{1,0:T(8,128)(2,1)...) custom-call(bf16[2048,256]{1,0:T(8,128)(2,1)} %refs_0_.1, ...), custom_call_target="tpu_custom_call" | custom-call | tf_op jit(solution)/shard_map/pallas_call | solution.py:342
  95.0 0.0 copy-start.4
  95.0 0.0 copy-start.11
  95.0 0.0 copy-start.10
  95.0 0.0 copy-start.1
  95.0 2.4 %copy.46 = f32[512,512]{1,0:T(8,128)} copy(f32[512,512]{1,0:T(8,128)} %get-tuple-element.30) | data formatting | bytes 2097152
  97.4 0.0 copy-done.4
  97.5 1.0 copy.47
  98.4 0.6 copy.48
  99.1 0.6 copy.49
  99.7 0.0 copy-done.1
  99.7 1.3 %copy.50 = bf16[2048,512]{1,0:T(8,128)(2,1)} copy(bf16[2048,512]{1,0:T(8,128)(2,1)S(1)} %copy-done.1) | data formatting | bytes 4194304
  101.0 0.6 copy-done.3
  101.7 1.0 copy.51
  102.6 1.0 copy.52
  103.6 0.6 copy.53
  104.2 0.6 copy.54
  104.9 1.3 %copy.55 = bf16[2048,512]{1,0:T(8,128)(2,1)} copy(bf16[2048,512]{1,0:T(8,128)(2,1)S(1)} %copy-done) | data formatting | bytes 4194304
  106.2 0.7 copy.56
  106.9 0.0 copy-done.6
  106.9 0.7 copy.57
  107.6 0.6 copy.58
  108.2 0.6 copy.59
  108.8 0.8 copy.60
  (20 shorter events, 0.0 us)
Async XLA Ops:
  95.0 2.5 %copy-start.4 = (f32[512,512]{1,0:T(8,128)S(1)}, f32[512,512]{1,0:T(8,128)}, u32[]{:S(2)}) copy-start(f32[512,512]{1,0:T(8,128)} %get-tuple-element.31) | copy-start | bytes 3145732
  95.0 3.4 %copy-start.11 = (f32[32,512]{1,0:T(8,128)S(1)}, f32[32,512]{1,0:T(8,128)}, u32[]{:S(2)}) copy-start(f32[32,512]{1,0:T(8,128)} %get-tuple-element.32) | copy-start | bytes 196612
  95.0 4.0 %copy-start.10 = (f32[32,512]{1,0:T(8,128)S(1)}, f32[32,512]{1,0:T(8,128)}, u32[]{:S(2)}) copy-start(f32[32,512]{1,0:T(8,128)} %get-tuple-element.33) | copy-start | bytes 196612
  95.0 4.7 %copy-start.1 = (bf16[2048,512]{1,0:T(8,128)(2,1)S(1)}, bf16[2048,512]{1,0:T(8,128)(2,1)}, u32[]{:S(2)}) copy-start(bf16[2048,512]{1,0:T(8,128)(2,1)} %get-tuple-element.34) | copy-start | bytes 6291460
  99.7 2.0 %copy-start.3 = (f32[512,512]{1,0:T(8,128)S(1)}, f32[512,512]{1,0:T(8,128)}, u32[]{:S(2)}) copy-start(f32[512,512]{1,0:T(8,128)} %get-tuple-element.35) | copy-start | bytes 3145732
  99.7 2.9 %copy-start.2 = (f32[512,512]{1,0:T(8,128)S(1)}, f32[512,512]{1,0:T(8,128)}, u32[]{:S(2)}) copy-start(f32[512,512]{1,0:T(8,128)} %get-tuple-element.36) | copy-start | bytes 3145732
  101.6 2.0 %copy-start.9 = (f32[32,512]{1,0:T(8,128)S(1)}, f32[32,512]{1,0:T(8,128)}, u32[]{:S(2)}) copy-start(f32[32,512]{1,0:T(8,128)} %get-tuple-element.37) | copy-start | bytes 196612
  101.7 2.6 %copy-start.8 = (f32[32,512]{1,0:T(8,128)S(1)}, f32[32,512]{1,0:T(8,128)}, u32[]{:S(2)}) copy-start(f32[32,512]{1,0:T(8,128)} %get-tuple-element.38) | copy-start | bytes 196612
  101.7 3.2 %copy-start = (bf16[2048,512]{1,0:T(8,128)(2,1)S(1)}, bf16[2048,512]{1,0:T(8,128)(2,1)}, u32[]{:S(2)}) copy-start(bf16[2048,512]{1,0:T(8,128)(2,1)} %get-tuple-element.39) | copy-start | bytes 6291460
  104.9 1.4 %copy-start.7 = (f32[512,128]{1,0:T(8,128)S(1)}, f32[512,128]{1,0:T(8,128)}, u32[]{:S(2)}) copy-start(f32[512,128]{1,0:T(8,128)} %get-tuple-element.40) | copy-start | bytes 786436
  104.9 2.1 %copy-start.6 = (f32[512,128]{1,0:T(8,128)S(1)}, f32[512,128]{1,0:T(8,128)}, u32[]{:S(2)}) copy-start(f32[512,128]{1,0:T(8,128)} %get-tuple-element.41) | copy-start | bytes 786436
  104.9 2.8 %copy-start.13 = (f32[32,128]{1,0:T(8,128)S(1)}, f32[32,128]{1,0:T(8,128)}, u32[]{:S(2)}) copy-start(f32[32,128]{1,0:T(8,128)} %get-tuple-element.42) | copy-start | bytes 49156
  104.9 3.4 %copy-start.12 = (f32[32,128]{1,0:T(8,128)S(1)}, f32[32,128]{1,0:T(8,128)}, u32[]{:S(2)}) copy-start(f32[32,128]{1,0:T(8,128)} %get-tuple-element.43) | copy-start | bytes 49156
  104.9 4.0 %copy-start.5 = (bf16[2048,128]{1,0:T(8,128)(2,1)S(1)}, bf16[2048,128]{1,0:T(8,128)(2,1)}, u32[]{:S(2)}) copy-start(bf16[2048,128]{1,0:T(8,128)(2,1)} %get-tuple-element.44) | copy-start | bytes 1572868

commit v2 on v1

--- a/solution.py
+++ b/solution.py
@@ -10,20 +10,21 @@
 MESH = pl.DeviceIdType.MESH
 PIECES = 4
 SKEW = 2
+AFTER = (0, 1, 4, 7, 9, 13)
 F32, BF16 = jnp.float32, jnp.bfloat16
 
 
 def kernel(n, tp, *refs):
     feat_in = refs[0]
     cot_in, basis_in, master_in, first_in, second_in = (refs[1 + i : 16 : 5] for i in range(5))
-    upd_out, mas_out, fir_out, sec_out, cop_out = (refs[16 + i : 31 : 5] for i in range(5))
+    upd, mas, fir, sec, cop = (refs[16 + i : 31 : 5] for i in range(5))
     (feat, fsib, cot, basis, master, first, second, parts, up_in, dn_in, up_snd, dn_snd,
-     tot, sib, proj, rs_in, direction, sums, upd, mas, fir, sec, cop,
-     load_sem, store_sem, z_send, z_recv, sib_send, sib_recv, rs_send, rs_recv,
+     tot, sib, proj, rs_in, direction, sums,
+     load_sem, z_send, z_recv, sib_send, sib_recv, rs_send, rs_recv,
      ag_send, ag_recv, sq_send, sq_recv, bulk_send, bulk_recv) = (
         refs[31], refs[32], refs[33:36], refs[36:39], refs[39:42], refs[42:45], refs[45:48],
         *refs[48:53], refs[53], refs[54], refs[55:58], refs[58:61], refs[61:64], refs[64],
-        refs[65:68], refs[68:71], refs[71:74], refs[74:77], refs[77:80], *refs[80:])
+        *refs[65:])
 
     f, t = lax.axis_index("fs"), lax.axis_index("tp")
     zs = tp // 2
@@ -36,7 +37,6 @@
     rb = rank // n
     piece = half // PIECES
     count = 3 * PIECES
-    sends = []
 
     def remote(src, dst, ssem, rsem, **dev):
         return pltpu.make_async_remote_copy(
@@ -145,11 +145,6 @@
         for d in range(1, n):
             rs_copy(k, d).start()
 
-    def store(src, dst, k, i):
-        cp = pltpu.make_async_copy(src, dst, store_sem.at[k, i])
-        cp.start()
-        sends.append(cp.wait)
-
     def act_moment(k):
         loads[7 + k].wait()
         loads[10 + k].wait()
@@ -164,8 +159,6 @@
         direction[k][rows_of(f), :] = a / jnp.sqrt(b)
         for d in range(1, n):
             ag_copy(k, d, f).start()
-        store(fir[k], fir_out[k], k, 0)
-        store(sec[k], sec_out[k], k, 1)
 
     rows = pl.ds(pl.multiple_of(f * rows_dev, rows_dev), rows_dev)
 
@@ -189,9 +182,6 @@
 
     def block(k, owner, h):
         return cop[k].at[pl.ds(pl.multiple_of(owner * rows_dev + h * hrow, hrow), hrow)]
-
-    def out_block(k, owner, h):
-        return cop_out[k].at[pl.ds(pl.multiple_of(owner * rows_dev + h * hrow, hrow), hrow)]
 
     x_peer = f + 1 - 2 * lax.rem(f, 2)
     y_peer = lax.rem(f + 2, 4)
@@ -221,10 +211,6 @@
             for d in range(1, n):
                 for h in range(2):
                     bulk(k, 2 * (d - 1) + h, f, h, lax.rem(f + d, n)).start()
-        store(upd[k], upd_out[k], k, 2)
-        store(mas[k], mas_out[k], k, 3)
-        for h in range(2):
-            store(block(k, f, h), out_block(k, f, h), k, 4 + h)
 
     def act_forward(k):
         if n == 4:
@@ -232,38 +218,32 @@
             bulk(k, 4, x_peer, 0, y_peer).start()
             bulk(k, 3, y_peer, 1, y_peer).wait_recv()
             bulk(k, 5, y_peer, 1, x_peer).start()
-            store(block(k, x_peer, 0), out_block(k, x_peer, 0), k, 6)
-            store(block(k, y_peer, 1), out_block(k, y_peer, 1), k, 7)
 
     def act_arrive(k):
         if n == 4:
             for i, (lane, owner, h) in enumerate(((1, x_peer, 1), (2, y_peer, 0), (4, diag, 0), (5, diag, 1))):
                 bulk(k, lane, owner, h, x_peer).wait_recv()
-                store(block(k, owner, h), out_block(k, owner, h), k, 8 + i)
         else:
             for d in range(1, n):
                 for h in range(2):
                     owner = lax.rem(f - d + n, n)
                     lane = 2 * (d - 1) + h
                     bulk(k, lane, owner, h, owner).wait_recv()
-                    store(block(k, owner, h), out_block(k, owner, h), k, 6 + lane)
 
     todo = {}
     for k in range(3):
         base = (k + 1) * PIECES - 1 + SKEW * (zs - 1)
-        for after, act in ((0, act_total), (1, act_project), (3, act_moment), (5, act_direction), (7, act_finish), (12, act_forward)):
+        for after, act in zip(AFTER, (act_total, act_project, act_moment, act_direction, act_finish, act_forward)):
             todo.setdefault(base + after, []).append((act, k))
     steps = count + SKEW * (zs - 1)
     for step in range(max(max(todo) + 1, steps)):
         if step < steps:
             z_step(step)
-        for act, k in todo.get(step, ()):
+        for act, k in sorted(todo.get(step, ()), key=lambda item: -item[1]):
             act(k)
     for k in range(3):
         act_arrive(k)
 
-    for wait in sends:
-        wait()
     for k in range(3):
         mate_copy[k].wait_send()
         for d in range(1, n):
@@ -306,11 +286,11 @@
     outs = []
     for k in range(3):
         outs += [
-            jax.ShapeDtypeStruct(masters[k].shape, F32),
-            jax.ShapeDtypeStruct(masters[k].shape, F32),
-            jax.ShapeDtypeStruct(firsts[k].shape, F32),
-            jax.ShapeDtypeStruct(firsts[k].shape, F32),
-            jax.ShapeDtypeStruct((whole_rows, cols[k]), BF16),
+            pltpu.VMEM(masters[k].shape, F32),
+            pltpu.VMEM(masters[k].shape, F32),
+            pltpu.VMEM(firsts[k].shape, F32),
+            pltpu.VMEM(firsts[k].shape, F32),
+            pltpu.VMEM((whole_rows, cols[k]), BF16),
         ]
     like = lambda arrays: [pltpu.VMEM(a.shape, a.dtype) for a in arrays]
     lanes = 6 if n == 4 else 2 * (n - 1)
@@ -329,12 +309,7 @@
         + [pltpu.VMEM((n - 1, rank // n, w), F32) for w in cols]
         + [pltpu.VMEM((rank, w), F32) for w in cols]
         + [pltpu.VMEM((3, tp, 8, 128), F32)]
-        + like(masters)
-        + like(masters)
-        + like(firsts)
-        + like(firsts)
-        + [pltpu.VMEM((whole_rows, w), BF16) for w in cols]
-        + [dma(16), dma(3, 6 + max(6, 2 * (n - 1))), dma(2, count), dma(2, count), dma(4), dma(4)]
+        + [dma(16), dma(2, count), dma(2, count), dma(4), dma(4)]
         + [dma(3, n - 1)] * 4
         + [dma(3, tp - 1)] * 2
         + [dma(3, lanes)] * 2
@@ -342,11 +317,11 @@
     return pl.pallas_call(
         functools.partial(kernel, n, tp),
         out_shape=outs,
-        in_specs=[pl.BlockSpec(memory_space=pl.ANY)] * 16,
-        out_specs=[pl.BlockSpec(memory_space=pl.ANY)] * 15,
+        in_specs=[pl.BlockSpec(memory_space=pltpu.HBM)] * 16,
+        out_specs=[pl.BlockSpec(memory_space=pltpu.VMEM)] * 15,
         scratch_shapes=scratch,
         compiler_params=pltpu.CompilerParams(
-            collective_id=0, has_side_effects=True, vmem_limit_bytes=60 * 1024 * 1024
+            collective_id=0, has_side_effects=True, vmem_limit_bytes=54 * 1024 * 1024
         ),
     )(*args)
 

time: 110 us -> 98.6 us (0.90)
  Pallas kernels: 94.3 us -> 85.4 us
  local copies, waits for them, and re-layouts: 14.6 us -> 12.4 us
    pallas_call x1, Pallas kernels: 94.3 us -> 85.4 us  [shards(): pl.pallas_call(functools.partial(kernel, n, tp), out_shape=outs, in_specs...]
    unnamed x43 -> x15, local copies, waits for them, and re-layouts: 14.6 us -> 12.4 us
where the time goes in v2:
time: 98.6 us; the launch traced here: 98.5 us
  Pallas kernels  85.4 us (87%)
  local copies, waits for them, and re-layouts  12.4 us (13%)
    pallas_call x1, Pallas kernels, shards(): pl.pallas_call(functools.partial(kernel, n, tp), out_shape=outs, in_specs...  85.4 us
    unnamed x15, local copies, waits for them, and re-layouts  12.4 us

profile of v2, /device:TPU:0, one launch (start us, length us, event | category | flops | bytes accessed | tf_op | source)
XLA Modules:
  0.0 98.5 jit_solution(17308926130512762032)
XLA Ops:
  0.7 85.4 %shard_map.271 = (f32[512,512]{1,0:T(8,128)S(1)}, f32[512,512]{1,0:T(8,128)S(1)}, f32[32,512]{1,0:T(8,128)S(1)}, f32[32,512]{1,0:T(8,128)S(1)}, bf16[2048,512]{1...) custom-call(bf16[2048,256]{1,0:T(8,128)(2,1)} %refs_0_.1, ...), custom_call_target="tpu_custom_call" | custom-call | tf_op jit(solution)/shard_map/pallas_call | solution.py:317
  86.0 1.0 copy.46
  87.0 0.6 copy.58
  87.6 0.6 copy.59
  88.2 0.6 copy.48
  88.8 0.6 copy.49
  89.5 0.6 copy.53
  90.1 0.6 copy.54
  90.7 0.7 copy.56
  91.4 0.7 copy.57
  92.1 0.8 copy.60
  92.9 1.0 copy.47
  93.9 1.0 copy.51
  94.9 1.0 copy.52
  95.8 1.3 %copy.50 = bf16[2048,512]{1,0:T(8,128)(2,1)} copy(bf16[2048,512]{1,0:T(8,128)(2,1)S(1)} %get-tuple-element.19) | data formatting | bytes 4194304
  97.2 1.3 %copy.55 = bf16[2048,512]{1,0:T(8,128)(2,1)} copy(bf16[2048,512]{1,0:T(8,128)(2,1)S(1)} %get-tuple-element.24) | data formatting | bytes 4194304
